TPU v7x, 32 devices: a whole 2x2x4 slice. The times are simulated.
32 devices in a mesh: fs: 8 (over z, x), tp: 4 (over y, core).
Axes of the slice: x: 2, y: 2, z: 4, core: 2. Of those that a mesh axis runs over, the one named last changes fastest.
Arguments:
- saved_input: bfloat16 [2048, 4096], P('fs'), may hold values from -8 to 8
- query_cotangent: bfloat16 [2048, 2048], P('fs', 'tp'), may hold values from -6 to 6
- layer_cotangent: bfloat16 [2048, 4096], P('fs'), may hold values from -8 to 8
- mixed_heads: bfloat16 [2048, 2048], P('fs', 'tp'), may hold values from -6 to 6
- query_basis: bfloat16 [4096, 256], P('fs'), may hold values from -0.125 to 0.125
- output_basis: bfloat16 [4096, 256], P('fs'), may hold values from -0.125 to 0.125
- query_master: float32 [4096, 2048], P('fs', 'tp'), may hold values from -3 to 3
- output_master: float32 [4096, 2048], P('fs', 'tp'), may hold values from -3 to 3
- query_first: float32 [256, 2048], P('fs', 'tp'), may hold values from -6 to 6
- query_second: float32 [256, 2048], P('fs', 'tp'), may hold values from 0.25 to 4
- output_first: float32 [256, 2048], P('fs', 'tp'), may hold values from -6 to 6
- output_second: float32 [256, 2048], P('fs', 'tp'), may hold values from 0.25 to 4
Outputs:
- query_weight: float32 [4096, 2048], P('fs', 'tp')
- output_weight: float32 [4096, 2048], P('fs', 'tp')
- query_step: float32 [4096, 2048], P('fs', 'tp')
- output_step: float32 [4096, 2048], P('fs', 'tp')
- query_first_new: float32 [256, 2048], P('fs', 'tp')
- query_second_new: float32 [256, 2048], P('fs', 'tp')
- output_first_new: float32 [256, 2048], P('fs', 'tp')
- output_second_new: float32 [256, 2048], P('fs', 'tp')
- query_copy: bfloat16 [4096, 2048], P(None, 'tp')
- output_copy: bfloat16 [4096, 2048], P(None, 'tp')
All inputs are finite; a program needn't handle non-finite values.
Results may differ from a plain program's by a relative error of at most 0.0028.
Values may be sent and summed in bfloat16 or wider, within the bound.
A program may use at most 64 MiB of HBM per device.

v0:
```python
import functools

import jax
import jax.numpy as jnp
from jax import lax
from jax.experimental import pallas as pl
from jax.experimental.pallas import tpu as pltpu
from jax.sharding import PartitionSpec as P

QW = 2048
RANK = 256


beta_one = 0.8
beta_two = 0.9
rate = 0.1


def moment_update(low, factor, first, second):
    scaled = low * factor
    first_new = beta_one * first + (1.0 - beta_one) * scaled
    second_new = beta_two * second + (1.0 - beta_two) * scaled * scaled
    direction = (first_new / jnp.sqrt(second_new)).astype(jnp.bfloat16)
    return (first_new, second_new, direction)


def contract_tokens(left, right):
    return lax.dot_general(
        left,
        right,
        (((0,), (0,)), ((), ())),
        precision=lax.Precision.HIGHEST,
        preferred_element_type=jnp.float32,
    )


def per_device(
    saved_input,
    query_cotangent,
    layer_cotangent,
    mixed_heads,
    query_basis,
    output_basis,
    query_master,
    output_master,
    query_first,
    query_second,
    output_first,
    output_second,
):
    query_coords = jnp.dot(
        saved_input,
        lax.all_gather(query_basis, "fs", axis=0, tiled=True),
        preferred_element_type=jnp.float32,
    )
    output_coords = jnp.dot(
        layer_cotangent,
        lax.all_gather(output_basis, "fs", axis=0, tiled=True),
        preferred_element_type=jnp.float32,
    )
    query_part = contract_tokens(query_coords, query_cotangent.astype(jnp.float32))
    output_part = contract_tokens(output_coords, mixed_heads.astype(jnp.float32))
    query_low, output_low = (
        lax.psum_scatter(query_part, "fs", scatter_dimension=0, tiled=True),
        lax.psum_scatter(output_part, "fs", scatter_dimension=0, tiled=True),
    )
    local_squares = jnp.sum(query_low * query_low) + jnp.sum(output_low * output_low)
    total_squares = lax.psum(local_squares, ("fs", "tp"))
    factor = 1.0 / jnp.sqrt(1.0 + total_squares / (2.0 * RANK * QW))
    qf, qs, qdir = moment_update(query_low, factor, query_first, query_second)
    of, osec, odir = moment_update(output_low, factor, output_first, output_second)
    query_whole, output_whole = (
        lax.all_gather(qdir, "fs", axis=0, tiled=True),
        lax.all_gather(odir, "fs", axis=0, tiled=True),
    )
    query_step = jnp.dot(query_basis, query_whole, preferred_element_type=jnp.float32)
    output_step = jnp.dot(output_basis, output_whole, preferred_element_type=jnp.float32)
    query_weight = query_master - rate * query_step
    output_weight = output_master - rate * output_step
    query_copy, output_copy = (
        lax.all_gather(query_weight.astype(jnp.bfloat16), "fs", axis=0, tiled=True),
        lax.all_gather(output_weight.astype(jnp.bfloat16), "fs", axis=0, tiled=True),
    )
    return (
        query_weight,
        output_weight,
        query_step,
        output_step,
        qf,
        qs,
        of,
        osec,
        query_copy,
        output_copy,
    )

MESH = pl.DeviceIdType.MESH
CHUNKS = 4


def ring_kernel(n, m, *refs):
    x_hbm, cot_hbm, basis_hbm, master_hbm, first_hbm, second_hbm = (
        (refs[0], refs[2]),
        (refs[1], refs[3]),
        (refs[4], refs[5]),
        (refs[6], refs[7]),
        (refs[8], refs[10]),
        (refs[9], refs[11]),
    )
    w_out, step_out, first_out, second_out, gathered = (
        (refs[12], refs[13]),
        (refs[14], refs[15]),
        (refs[16], refs[18]),
        (refs[17], refs[19]),
        (refs[20], refs[21]),
    )
    (
        x_v, cot_v, basis, master_v, first, second,
        rows_v, ahead_v, wide_v, flat_v, coord_v, part_v, pair_v, got_v, square_v, direction_v,
        in_sem, rows_sem, coord_sem, pair_sem, part_sem, square_sem, direction_sem, gather_sem, ahead_sem, wide_sem,
    ) = refs[22:]
    f, t = lax.axis_index("fs"), lax.axis_index("tp")
    me = f * m + t
    rank_part, block = rows_v.shape[2:]
    piece = block // CHUNKS
    rank = basis.shape[2]
    tokens = x_v.shape[1]
    columns = cot_v.shape[2]
    low_rows = first.shape[1]
    half = n // 2
    z, x = f // 2, lax.rem(f, 2)
    across = z * 2 + 1 - x

    def along(d, side=None):
        side = x if side is None else side
        return lax.rem(z + d + half, half) * 2 + side

    loads = {}
    for k in range(2):
        loads["basis", k] = pltpu.make_async_copy(basis_hbm[k], basis.at[k], in_sem.at[0, k])
    for i, (name, sources, target) in enumerate(
        (
            ("x", x_hbm, x_v),
            ("cot", cot_hbm, cot_v),
            ("first", first_hbm, first),
            ("second", second_hbm, second),
            ("master", master_hbm, master_v),
        )
    ):
        for k in range(2):
            loads[name, k] = pltpu.make_async_copy(sources[k], target.at[k], in_sem.at[1 + i, k])
    for copy in loads.values():
        copy.start()

    barrier = pltpu.get_barrier_semaphore()
    for d in range(1, n * m):
        other = lax.rem(me + d, n * m)
        pl.semaphore_signal(barrier, inc=1, device_id={"fs": other // m, "tp": lax.rem(other, m)}, device_id_type=MESH)

    chosen = lax.broadcasted_iota(jnp.int32, (rank_part, rank), 1) == (
        lax.broadcasted_iota(jnp.int32, (rank_part, rank), 0) + t * rank_part
    )
    select = jnp.where(chosen, 1.0, 0.0).astype(jnp.bfloat16)
    for k in range(2):
        loads["basis", k].wait()
        rows_v[k, 0] = lax.dot_general(
            select, basis[k], (((1,), (1,)), ((), ())), preferred_element_type=jnp.float32
        ).astype(jnp.bfloat16)
    pl.semaphore_wait(barrier, n * m - 1)

    sent = []

    def send(source, target, sems, index, device):
        copy = pltpu.make_async_remote_copy(
            src_ref=source,
            dst_ref=target,
            send_sem=sems.at[(0,) + index],
            recv_sem=sems.at[(1,) + index],
            device_id=device,
            device_id_type=MESH,
        )
        copy.start()
        sent.append(copy)
        return copy

    def push(own, slots, sems, k):
        copies = {half: send(own, slots(half), sems, (k, half), {"fs": across})}
        for d in (1, half - 1, *range(2, half - 1)):
            copies[d] = send(own, slots(d), sems, (k, d), {"fs": along(d)})
        return copies

    def relay(copies, slots, sems, k):
        for d in (1, half - 1, *range(2, half - 1)):
            copies[d].wait_recv()
            copies[half + d] = send(slots(d), slots(half + d), sems, (k, half + d), {"fs": across})

    def rows_at(k):
        return lambda d: rows_v.at[k, d]

    rows = [push(rows_v.at[k, 0], rows_at(k), rows_sem, k) for k in range(2)]

    def coordinates(k, d):
        source = along(-(d % half), x if d < half else 1 - x)
        left = rows_v[k, d]
        right = x_v[k, :, pl.ds(pl.multiple_of(source * block, block), block)]
        return lax.dot_general(left, right, (((1,), (1,)), ((), ())), preferred_element_type=jnp.float32)

    def ahead_at(k):
        return lambda d: ahead_v.at[k, d]

    coords, ahead = [], []
    for k in range(2):
        if k == 0:
            relay(rows[0], rows_at(0), rows_sem, 0)
        loads["x", k].wait()
        total = coordinates(k, 0)
        for d in range(1, half):
            total = total + coordinates(k, d)
        if k == 0:
            relay(rows[1], rows_at(1), rows_sem, 1)
            for i in range(2):
                loads["master", i].wait()
                ahead_v[i, 0] = master_v[i, pl.ds(0, piece)].astype(jnp.bfloat16)
                ahead.append(push(ahead_v.at[i, 0], ahead_at(i), ahead_sem, i))
        for d in range(half, n):
            rows[k][d].wait_recv()
            total = total + coordinates(k, d)
        high = total.astype(jnp.bfloat16)
        coord_v[k, t, 0] = high
        coord_v[k, t, 1] = (total - high.astype(jnp.float32)).astype(jnp.bfloat16)
        coords.append(
            [
                send(coord_v.at[k, t], coord_v.at[k, t], coord_sem, (k, d), {"tp": lax.rem(t + d, m)})
                for d in range(1, m)
            ]
        )

    wide = []
    for k in range(2):
        source = rows_v.at[k, :, :, pl.ds(0, piece)]
        for d in range(1, m):
            wide.append(send(source, wide_v.at[k, t], wide_sem, (k, d), {"tp": lax.rem(t + d, m)}))
        wide_v[k, t] = rows_v[k, :, :, :piece]
    pairs = []
    for k in range(2):
        loads["cot", k].wait()
        for copy in coords[k]:
            copy.wait_recv()
        part = jnp.dot(
            coord_v[k, :, 0].reshape(rank, tokens), cot_v[k], preferred_element_type=jnp.float32
        ) + jnp.dot(coord_v[k, :, 1].reshape(rank, tokens), cot_v[k], preferred_element_type=jnp.float32)
        part_v[k] = part.reshape(n, low_rows, columns)
        pairs.append({})
        for d in (1, half - 1, *range(2, half - 1), 0):
            pairs[k][d] = send(
                part_v.at[k, along(d, 1 - x)], pair_v.at[k, d], pair_sem, (k, d), {"fs": across}
            )
    parts = []
    for k in range(2):
        parts.append({})
        for d in (1, half - 1, *range(2, half - 1)):
            pairs[k][d].wait_recv()
            pair_v[k, d] = pair_v[k, d] + part_v[k, along(d)]
            parts[k][d] = send(pair_v.at[k, d], got_v.at[k, d], part_sem, (k, d), {"fs": along(d)})
        relay(ahead[k], ahead_at(k), ahead_sem, k)

    lows = []
    squares = jnp.zeros((), jnp.float32)
    for k in range(2):
        pairs[k][0].wait_recv()
        low = pair_v[k, 0] + part_v[k, f]
        for d in range(1, half):
            parts[k][d].wait_recv()
            low = low + got_v[k, d]
        lows.append(low)
        squares = squares + jnp.sum(low * low)
    square_v[0] = jnp.full(square_v.shape[1:], squares, jnp.float32)
    copies = []
    for d in range(1, n * m):
        other = lax.rem(me + d, n * m)
        copies.append(
            send(square_v.at[0], square_v.at[d], square_sem, (d,), {"fs": other // m, "tp": lax.rem(other, m)})
        )
    for copy in wide:
        copy.wait_recv()
    for k in range(2):
        for d in range(n):
            flat_v[k, d] = wide_v[k, :, d].reshape(rank, piece).T
    for k in range(2):
        loads["first", k].wait()
        loads["second", k].wait()
    for copy in copies:
        copy.wait_recv()
    total_squares = jnp.sum(square_v[...], axis=0)[:1, :1]
    factor = 1.0 / jnp.sqrt(1.0 + total_squares / (2.0 * rank * (columns * m)))

    directions = []
    for k in range(2):
        new_first, new_second, direction = moment_update(lows[k], factor, first[k], second[k])
        direction_v[k, f] = direction
        own = direction_v.at[k, f]
        directions.append(push(own, lambda d: own, direction_sem, k))
        first_out[k][...] = new_first
        second_out[k][...] = new_second
    for k in range(2):
        for d in (1, half - 1, *range(2, half - 1)):
            directions[k][d].wait_recv()
            arrived = direction_v.at[k, along(-d)]
            directions[k][half + d] = send(arrived, arrived, direction_sem, (k, half + d), {"fs": across})

    place = (1 - x) * z + x * (n - 1 - z)

    def at(p):
        p = lax.rem(p + 2 * n, n)
        h = p // half
        return (1 - h) * 2 * p + h * (2 * (n - 1 - p) + 1)

    toward = (at(place + 1), at(place - 1))
    origin = [[at(place - s), at(place + s)] for s in range(n)]
    for k in range(2):
        for d in range(half, n):
            directions[k][d].wait_recv()
    ring = {}

    def forward(s, k, c):
        where = gathered[k].at[pl.ds(pl.multiple_of(origin[s][k] * block + c * piece, piece), piece)]
        ring[s, k, c] = send(where, where, gather_sem, (k, s, c), {"fs": toward[k]})

    def own_piece(c):
        for k in range(2):
            span = pl.ds(c * piece, piece)
            step = jnp.dot(
                basis[k, span, :],
                direction_v[k].reshape(rank, columns),
                preferred_element_type=jnp.float32,
            )
            weight = master_v[k, span, :] - rate * step
            if c > 0:
                gathered[k][pl.ds(pl.multiple_of(f * block + c * piece, piece), piece)] = weight.astype(jnp.bfloat16)
                forward(0, k, c)
            step_out[k][span] = step
            w_out[k][span] = weight
    def finish_ahead(k, d):
        source = along(-(d % half), x if d < half else 1 - x)
        if d >= half:
            ahead[k][d].wait_recv()
        step = jnp.dot(
            flat_v[k, d], direction_v[k].reshape(rank, columns), preferred_element_type=jnp.float32
        )
        weight = ahead_v[k, d].astype(jnp.float32) - rate * step
        gathered[k][pl.ds(pl.multiple_of(source * block, block), piece)] = weight.astype(jnp.bfloat16)

    for c in (*range(1, CHUNKS), 0):
        own_piece(c)
    units = [(k, d) for d in range(n) for k in range(2)]
    for s in range(1, n):
        for c in range(1, CHUNKS):
            for k in range(2):
                ring[s - 1, k, c].wait_recv()
                if s < n - 1:
                    forward(s, k, c)
            if units:
                finish_ahead(*units.pop(0))
    for unit in units:
        finish_ahead(*unit)
    for copy in sent:
        copy.wait_send()


def write_kernel(count, *refs):
    sem = refs[2 * count]
    copies = [pltpu.make_async_copy(refs[i], refs[count + i], sem.at[i]) for i in range(count)]
    for copy in copies:
        copy.start()
    for copy in copies:
        copy.wait()


def fused_per_device(n, m, *args):
    x, cot, _, _, basis = args[:5]
    first = args[8]
    block, rank = basis.shape
    columns = cot.shape[1]
    tokens, width = x.shape
    part = rank // m
    low_rows = first.shape[0]
    bf16, f32 = jnp.bfloat16, jnp.float32
    kinds = [((block, columns), f32)] * 4 + [(first.shape, f32)] * 4 + [((width, columns), bf16)] * 2
    hbm = pl.BlockSpec(memory_space=pltpu.HBM)
    vmem = pl.BlockSpec(memory_space=pltpu.VMEM)
    dma = pltpu.SemaphoreType.DMA
    results = pl.pallas_call(
        functools.partial(ring_kernel, n, m),
        out_shape=tuple(pltpu.VMEM(*kind) for kind in kinds),
        in_specs=[hbm] * 12,
        out_specs=(vmem,) * 10,
        scratch_shapes=[
            pltpu.VMEM((2, tokens, width), bf16),
            pltpu.VMEM((2, tokens, columns), bf16),
            pltpu.VMEM((2, block, rank), bf16),
            pltpu.VMEM((2, block, columns), f32),
            pltpu.VMEM((2, low_rows, columns), f32),
            pltpu.VMEM((2, low_rows, columns), f32),
            pltpu.VMEM((2, n, part, block), bf16),
            pltpu.VMEM((2, n, block // CHUNKS, columns), bf16),
            pltpu.VMEM((2, m, n, part, block // CHUNKS), bf16),
            pltpu.VMEM((2, n, block // CHUNKS, rank), bf16),
            pltpu.VMEM((2, m, 2, part, tokens), bf16),
            pltpu.VMEM((2, n, low_rows, columns), f32),
            pltpu.VMEM((2, n // 2, low_rows, columns), f32),
            pltpu.VMEM((2, n // 2, low_rows, columns), f32),
            pltpu.VMEM((n * m, 8, 128), f32),
            pltpu.VMEM((2, n, low_rows, columns), bf16),
            dma((6, 2)),
            dma((2, 2, n)),
            dma((2, 2, m)),
            dma((2, 2, n // 2)),
            dma((2, 2, n // 2)),
            dma((2, n * m)),
            dma((2, 2, n)),
            dma((2, 2, n - 1, CHUNKS)),
            dma((2, 2, n)),
            dma((2, 2, m)),
        ],
        compiler_params=pltpu.CompilerParams(
            collective_id=0, has_side_effects=True, vmem_limit_bytes=48 * 2**20
        ),
    )(*args)
    return pl.pallas_call(
        functools.partial(write_kernel, len(kinds)),
        out_shape=tuple(jax.ShapeDtypeStruct(*kind) for kind in kinds),
        in_specs=[pl.BlockSpec(memory_space=pl.ANY)] * len(kinds),
        out_specs=(hbm,) * len(kinds),
        scratch_shapes=[dma((len(kinds),))],
        compiler_params=pltpu.CompilerParams(vmem_limit_bytes=2**20),
    )(*results)


def fits(n, m, *args):
    basis, first = args[4], args[8]
    return (
        n % 2 == 0
        and basis.shape[1] // n % 16 == 0
        and basis.shape[1] // m % 16 == 0
        and basis.shape[0] // n % (128 * CHUNKS) == 0
        and basis.shape[0] // n % 128 == 0
        and first.shape[1] // m % 128 == 0
    )


def solution(mesh):
    placed = (
        P("fs", None),
        P("fs", "tp"),
        P("fs", None),
        P("fs", "tp"),
        P("fs", None),
        P("fs", None),
        P("fs", "tp"),
        P("fs", "tp"),
        P("fs", "tp"),
        P("fs", "tp"),
        P("fs", "tp"),
        P("fs", "tp"),
    )
    n, m = mesh.shape["fs"], mesh.shape["tp"]

    def step(*args):
        body = functools.partial(fused_per_device, n, m) if fits(n, m, *args) else per_device
        return jax.shard_map(
            body,
            mesh=mesh,
            in_specs=placed,
            out_specs=(P("fs", "tp"),) * 8 + (P(None, "tp"),) * 2,
            check_vma=False,
        )(*args)

    return step
```

profile of v0, /device:TPU:0, one launch (start us, length us, event | category | flops | bytes accessed | tf_op | source)
XLA Modules:
  0.0 138.2 jit_solution(8725757504756499722)
XLA Ops:
  0.6 132.7 %shard_map.195 = (f32[512,512]{1,0:T(8,128)S(1)}, f32[512,512]{1,0:T(8,128)S(1)}, f32[512,512]{1,0:T(8,128)S(1)}, f32[512,512]{1,0:T(8,128)S(1)}, f32[32,512]{1,...) custom-call(bf16[256,4096]{1,0:T(8,128)(2,1)} %refs_0_.1, ...), custom_call_target="tpu_custom_call" | custom-call | tf_op jit(solution)/shard_map/pallas_call | solution.py:392
  133.4 4.8 %shard_map.196 = (f32[512,512]{1,0:T(8,128)}, f32[512,512]{1,0:T(8,128)}, f32[512,512]{1,0:T(8,128)}, f32[512,512]{1,0:T(8,128)}, f32[32,512]{1,0:T(8,128)}, /*i...) custom-call(f32[512,512]{1,0:T(8,128)S(1)} %get-tuple-element.20.ref, ...), custom_call_target="tpu_custom_call" | custom-call | tf_op jit(solution)/shard_map/pallas_call | solution.py:429
where the time goes:
time: 138 us
  Pallas kernels  138 us (100%)
    pallas_call x1, Pallas kernels, fused_per_device(): pl.pallas_call(functools.partial(ring_kernel, n, m), out_shape=tuple((plt...  133 us
    pallas_call x1, Pallas kernels, fused_per_device(): pl.pallas_call(functools.partial(write_kernel, len(kinds)), out_shape=tup...  4.83 us

commit v1 on v0

--- a/solution.py
+++ b/solution.py
@@ -95,7 +95,34 @@
     )
 
 MESH = pl.DeviceIdType.MESH
-CHUNKS = 4
+PIECES = 8
+FLIGHT = 4
+PACE = (4, 2, 2, 3, 3, 3, 3, 3, 3, 8, 6, 4)
+STRETCH = 40.0
+REACH = 3.0
+LN2 = 0.6931471805599453
+
+
+def encode(value):
+    size = jnp.abs(value) * STRETCH
+    small = size * LN2
+    near = small * (1.0 + small * (0.5 + small * (1.0 / 6.0)))
+    code = jnp.where(small < 0.02, near, jnp.exp2(size) - 1.0)
+    return jnp.where(value < 0.0, -code, code).astype(jnp.bfloat16)
+
+
+def decode(code):
+    code = code.astype(jnp.float32)
+    size = jnp.abs(code)
+    near = size * (1.0 - size * (0.5 - size * (1.0 / 3.0)))
+    value = jnp.where(size < 0.02, near, jnp.log(1.0 + size)) * (1.0 / (LN2 * STRETCH))
+    return jnp.where(code < 0.0, -value, value)
+
+
+def encode_scaled(value):
+    peak = jnp.max(jnp.max(jnp.abs(value), axis=1, keepdims=True), axis=0, keepdims=True)
+    unit = jnp.maximum(peak, 1e-30) * (1.0 / REACH)
+    return encode(value / unit), unit
 
 
 def ring_kernel(n, m, *refs):
@@ -116,13 +143,14 @@
     )
     (
         x_v, cot_v, basis, master_v, first, second,
-        rows_v, ahead_v, wide_v, flat_v, coord_v, part_v, pair_v, got_v, square_v, direction_v,
-        in_sem, rows_sem, coord_sem, pair_sem, part_sem, square_sem, direction_sem, gather_sem, ahead_sem, wide_sem,
+        rows_v, code_v, wide_v, flat_v, coord_v, part_v, mine_v, pair_v, sum_v, got_v, unit_v,
+        square_v, direction_v,
+        in_sem, rows_sem, coord_sem, pair_sem, part_sem, unit_sem, square_sem, direction_sem, ring_sem, wide_sem,
     ) = refs[22:]
     f, t = lax.axis_index("fs"), lax.axis_index("tp")
     me = f * m + t
     rank_part, block = rows_v.shape[2:]
-    piece = block // CHUNKS
+    piece = block // PIECES
     rank = basis.shape[2]
     tokens = x_v.shape[1]
     columns = cot_v.shape[2]
@@ -130,25 +158,29 @@
     half = n // 2
     z, x = f // 2, lax.rem(f, 2)
     across = z * 2 + 1 - x
+    partner, opposite = t + 1 - 2 * lax.rem(t, 2), lax.rem(t + m // 2, m)
+    order = (1, half - 1, *range(2, half - 1))
 
     def along(d, side=None):
         side = x if side is None else side
         return lax.rem(z + d + half, half) * 2 + side
 
+    def source_of(d):
+        return along(-(d % half), x if d < half else 1 - x)
+
     loads = {}
-    for k in range(2):
-        loads["basis", k] = pltpu.make_async_copy(basis_hbm[k], basis.at[k], in_sem.at[0, k])
     for i, (name, sources, target) in enumerate(
         (
+            ("basis", basis_hbm, basis),
+            ("master", master_hbm, master_v),
             ("x", x_hbm, x_v),
             ("cot", cot_hbm, cot_v),
             ("first", first_hbm, first),
             ("second", second_hbm, second),
-            ("master", master_hbm, master_v),
         )
     ):
         for k in range(2):
-            loads[name, k] = pltpu.make_async_copy(sources[k], target.at[k], in_sem.at[1 + i, k])
+            loads[name, k] = pltpu.make_async_copy(sources[k], target.at[k], in_sem.at[i, k])
     for copy in loads.values():
         copy.start()
 
@@ -166,7 +198,8 @@
         rows_v[k, 0] = lax.dot_general(
             select, basis[k], (((1,), (1,)), ((), ())), preferred_element_type=jnp.float32
         ).astype(jnp.bfloat16)
-    pl.semaphore_wait(barrier, n * m - 1)
+    with jax.named_scope("barrier"):
+        pl.semaphore_wait(barrier, n * m - 1)
 
     sent = []
 
@@ -185,45 +218,76 @@
 
     def push(own, slots, sems, k):
         copies = {half: send(own, slots(half), sems, (k, half), {"fs": across})}
-        for d in (1, half - 1, *range(2, half - 1)):
+        for d in order:
             copies[d] = send(own, slots(d), sems, (k, d), {"fs": along(d)})
         return copies
 
     def relay(copies, slots, sems, k):
-        for d in (1, half - 1, *range(2, half - 1)):
-            copies[d].wait_recv()
+        for d in order:
+            with jax.named_scope(f"rows_wait#k={k}#d={d}"):
+                copies[d].wait_recv()
             copies[half + d] = send(slots(d), slots(half + d), sems, (k, half + d), {"fs": across})
+
+    place = (1 - x) * z + x * (n - 1 - z)
+
+    def at(p):
+        p = lax.rem(p + 2 * n, n)
+        h = p // half
+        return (1 - h) * 2 * p + h * (2 * (n - 1 - p) + 1)
+
+    toward = (at(place + 1), at(place - 1))
+    origin = [[at(place - s), at(place + s)] for s in range(n)]
+    ring = {}
+    slots = [
+        (s, g * FLIGHT + w) for g in range(PIECES // FLIGHT) for s in range(n) for w in range(FLIGHT)
+    ]
+    arrived = []
+
+    def advance(count):
+        for _ in range(min(count, len(slots))):
+            s, c = slots.pop(0)
+            for k in range(2):
+                if s > 0:
+                    with jax.named_scope(f"ring_wait#s={s}#c={c}#k={k}"):
+                        ring[s - 1, k, c].wait_recv()
+                if s < n - 1:
+                    where = code_v.at[k, origin[s][k], pl.ds(c * piece, piece)]
+                    ring[s, k, c] = send(where, where, ring_sem, (k, s, c), {"fs": toward[k]})
+            if s > 0:
+                arrived.append((s, c))
+
+    pace = list(PACE)
 
     def rows_at(k):
         return lambda d: rows_v.at[k, d]
 
     rows = [push(rows_v.at[k, 0], rows_at(k), rows_sem, k) for k in range(2)]
+    for i in range(PIECES // FLIGHT):
+        span = pl.ds(i * FLIGHT * piece, FLIGHT * piece)
+        for k in range(2):
+            if i == 0:
+                loads["master", k].wait()
+            code_v[k, f, span] = encode(master_v[k, span])
+        if i == 0:
+            advance(pace.pop(0))
 
     def coordinates(k, d):
-        source = along(-(d % half), x if d < half else 1 - x)
         left = rows_v[k, d]
-        right = x_v[k, :, pl.ds(pl.multiple_of(source * block, block), block)]
+        right = x_v[k, :, pl.ds(pl.multiple_of(source_of(d) * block, block), block)]
         return lax.dot_general(left, right, (((1,), (1,)), ((), ())), preferred_element_type=jnp.float32)
 
-    def ahead_at(k):
-        return lambda d: ahead_v.at[k, d]
-
-    coords, ahead = [], []
-    for k in range(2):
-        if k == 0:
-            relay(rows[0], rows_at(0), rows_sem, 0)
+    for k in range(2):
+        relay(rows[k], rows_at(k), rows_sem, k)
+        advance(pace.pop(0))
+    coords = []
+    for k in range(2):
         loads["x", k].wait()
         total = coordinates(k, 0)
         for d in range(1, half):
             total = total + coordinates(k, d)
-        if k == 0:
-            relay(rows[1], rows_at(1), rows_sem, 1)
-            for i in range(2):
-                loads["master", i].wait()
-                ahead_v[i, 0] = master_v[i, pl.ds(0, piece)].astype(jnp.bfloat16)
-                ahead.append(push(ahead_v.at[i, 0], ahead_at(i), ahead_sem, i))
         for d in range(half, n):
-            rows[k][d].wait_recv()
+            with jax.named_scope(f"rows_late#k={k}#d={d}"):
+                rows[k][d].wait_recv()
             total = total + coordinates(k, d)
         high = total.astype(jnp.bfloat16)
         coord_v[k, t, 0] = high
@@ -234,44 +298,60 @@
                 for d in range(1, m)
             ]
         )
+        advance(pace.pop(0))
 
     wide = []
     for k in range(2):
-        source = rows_v.at[k, :, :, pl.ds(0, piece)]
-        for d in range(1, m):
-            wide.append(send(source, wide_v.at[k, t], wide_sem, (k, d), {"tp": lax.rem(t + d, m)}))
-        wide_v[k, t] = rows_v[k, :, :, :piece]
-    pairs = []
+        for target in (opposite, partner):
+            index = (k, len(wide) % 2)
+            wide.append(send(rows_v.at[k], wide_v.at[k, t], wide_sem, index, {"tp": target}))
+        wide_v[k, t] = rows_v[k]
+    pairs, units = [], []
     for k in range(2):
         loads["cot", k].wait()
-        for copy in coords[k]:
-            copy.wait_recv()
+        with jax.named_scope(f"coords_wait#k={k}"):
+            for copy in coords[k]:
+                copy.wait_recv()
         part = jnp.dot(
             coord_v[k, :, 0].reshape(rank, tokens), cot_v[k], preferred_element_type=jnp.float32
         ) + jnp.dot(coord_v[k, :, 1].reshape(rank, tokens), cot_v[k], preferred_element_type=jnp.float32)
         part_v[k] = part.reshape(n, low_rows, columns)
+        code, unit = encode_scaled(part)
+        mine_v[k] = code.reshape(n, low_rows, columns)
+        unit_v[0, k, 0] = jnp.broadcast_to(unit, unit_v.shape[3:])
         pairs.append({})
-        for d in (1, half - 1, *range(2, half - 1), 0):
+        units.append({0: send(unit_v.at[0, k, 0], unit_v.at[1, k, 0], unit_sem, (k, 0), {"fs": across})})
+        for d in (*order, 0):
             pairs[k][d] = send(
-                part_v.at[k, along(d, 1 - x)], pair_v.at[k, d], pair_sem, (k, d), {"fs": across}
+                mine_v.at[k, along(d, 1 - x)], pair_v.at[k, d], pair_sem, (k, d), {"fs": across}
             )
+        advance(pace.pop(0))
     parts = []
+    def paired(k, d):
+        with jax.named_scope(f"pair_wait#k={k}#d={d}"):
+            pairs[k][d].wait_recv()
+        return decode(pair_v[k, d]) * unit_v[1, k, 0][:1, :1] + part_v[k, along(d)]
+
     for k in range(2):
         parts.append({})
-        for d in (1, half - 1, *range(2, half - 1)):
-            pairs[k][d].wait_recv()
-            pair_v[k, d] = pair_v[k, d] + part_v[k, along(d)]
-            parts[k][d] = send(pair_v.at[k, d], got_v.at[k, d], part_sem, (k, d), {"fs": along(d)})
-        relay(ahead[k], ahead_at(k), ahead_sem, k)
+        units[k][0].wait_recv()
+        for d in order:
+            code, unit = encode_scaled(paired(k, d))
+            sum_v[k, d] = code
+            unit_v[0, k, d] = jnp.broadcast_to(unit, unit_v.shape[3:])
+            units[k][d] = send(unit_v.at[0, k, d], unit_v.at[1, k, d], unit_sem, (k, d), {"fs": along(d)})
+            parts[k][d] = send(sum_v.at[k, d], got_v.at[k, d], part_sem, (k, d), {"fs": along(d)})
+        advance(pace.pop(0))
 
     lows = []
     squares = jnp.zeros((), jnp.float32)
     for k in range(2):
-        pairs[k][0].wait_recv()
-        low = pair_v[k, 0] + part_v[k, f]
+        low = paired(k, 0)
         for d in range(1, half):
-            parts[k][d].wait_recv()
-            low = low + got_v[k, d]
+            with jax.named_scope(f"part_wait#k={k}#d={d}"):
+                units[k][d].wait_recv()
+                parts[k][d].wait_recv()
+            low = low + decode(got_v[k, d]) * unit_v[1, k, d][:1, :1]
         lows.append(low)
         squares = squares + jnp.sum(low * low)
     square_v[0] = jnp.full(square_v.shape[1:], squares, jnp.float32)
@@ -281,16 +361,13 @@
         copies.append(
             send(square_v.at[0], square_v.at[d], square_sem, (d,), {"fs": other // m, "tp": lax.rem(other, m)})
         )
-    for copy in wide:
-        copy.wait_recv()
-    for k in range(2):
-        for d in range(n):
-            flat_v[k, d] = wide_v[k, :, d].reshape(rank, piece).T
+    advance(pace.pop(0))
     for k in range(2):
         loads["first", k].wait()
         loads["second", k].wait()
-    for copy in copies:
-        copy.wait_recv()
+    with jax.named_scope("square_wait"):
+        for copy in copies:
+            copy.wait_recv()
     total_squares = jnp.sum(square_v[...], axis=0)[:1, :1]
     factor = 1.0 / jnp.sqrt(1.0 + total_squares / (2.0 * rank * (columns * m)))
 
@@ -302,69 +379,83 @@
         directions.append(push(own, lambda d: own, direction_sem, k))
         first_out[k][...] = new_first
         second_out[k][...] = new_second
-    for k in range(2):
-        for d in (1, half - 1, *range(2, half - 1)):
-            directions[k][d].wait_recv()
-            arrived = direction_v.at[k, along(-d)]
-            directions[k][half + d] = send(arrived, arrived, direction_sem, (k, half + d), {"fs": across})
-
-    place = (1 - x) * z + x * (n - 1 - z)
-
-    def at(p):
-        p = lax.rem(p + 2 * n, n)
-        h = p // half
-        return (1 - h) * 2 * p + h * (2 * (n - 1 - p) + 1)
-
-    toward = (at(place + 1), at(place - 1))
-    origin = [[at(place - s), at(place + s)] for s in range(n)]
+    advance(pace.pop(0))
+    for k in range(2):
+        wide[2 * k].wait_recv()
+        there = wide_v.at[k, opposite]
+        wide.append(send(there, there, wide_sem, (k, 2), {"tp": partner}))
+    for k in range(2):
+        for d in order:
+            with jax.named_scope(f"direction_wait#k={k}#d={d}"):
+                directions[k][d].wait_recv()
+            there = direction_v.at[k, along(-d)]
+            directions[k][half + d] = send(there, there, direction_sem, (k, half + d), {"fs": across})
+    advance(pace.pop(0))
+    with jax.named_scope("wide_wait"):
+        for copy in (wide[1], wide[3], wide[4], wide[5]):
+            copy.wait_recv()
+    for k in range(2):
+        for d in range(1, n):
+            flat_v[k, source_of(d)] = wide_v[k, :, d].reshape(rank, block).T
     for k in range(2):
         for d in range(half, n):
-            directions[k][d].wait_recv()
-    ring = {}
-
-    def forward(s, k, c):
-        where = gathered[k].at[pl.ds(pl.multiple_of(origin[s][k] * block + c * piece, piece), piece)]
-        ring[s, k, c] = send(where, where, gather_sem, (k, s, c), {"fs": toward[k]})
-
-    def own_piece(c):
-        for k in range(2):
-            span = pl.ds(c * piece, piece)
-            step = jnp.dot(
-                basis[k, span, :],
-                direction_v[k].reshape(rank, columns),
-                preferred_element_type=jnp.float32,
-            )
-            weight = master_v[k, span, :] - rate * step
-            if c > 0:
-                gathered[k][pl.ds(pl.multiple_of(f * block + c * piece, piece), piece)] = weight.astype(jnp.bfloat16)
-                forward(0, k, c)
-            step_out[k][span] = step
-            w_out[k][span] = weight
-    def finish_ahead(k, d):
-        source = along(-(d % half), x if d < half else 1 - x)
-        if d >= half:
-            ahead[k][d].wait_recv()
+            with jax.named_scope(f"direction_late#k={k}#d={d}"):
+                directions[k][d].wait_recv()
+
+    def own_rows(k, start, size):
+        span = pl.ds(start, size)
         step = jnp.dot(
-            flat_v[k, d], direction_v[k].reshape(rank, columns), preferred_element_type=jnp.float32
+            basis[k, span, :], direction_v[k].reshape(rank, columns), preferred_element_type=jnp.float32
         )
-        weight = ahead_v[k, d].astype(jnp.float32) - rate * step
-        gathered[k][pl.ds(pl.multiple_of(source * block, block), piece)] = weight.astype(jnp.bfloat16)
-
-    for c in (*range(1, CHUNKS), 0):
-        own_piece(c)
-    units = [(k, d) for d in range(n) for k in range(2)]
-    for s in range(1, n):
-        for c in range(1, CHUNKS):
+        weight = master_v[k, span, :] - rate * step
+        gathered[k][pl.ds(pl.multiple_of(f * block + start, size), size)] = weight.astype(jnp.bfloat16)
+        step_out[k][span] = step
+        w_out[k][span] = weight
+
+    def finish(k, s, start, size):
+        source = origin[s][k]
+        span = pl.ds(start, size)
+        step = jnp.dot(
+            flat_v[k, source, span, :],
+            direction_v[k].reshape(rank, columns),
+            preferred_element_type=jnp.float32,
+        )
+        weight = decode(code_v[k, source, span]) - rate * step
+        gathered[k][pl.ds(pl.multiple_of(source * block + start, size), size)] = weight.astype(jnp.bfloat16)
+
+    own = [(k, i * FLIGHT * piece) for i in range(PIECES // FLIGHT) for k in range(2)]
+    done = set()
+
+    def ready(limit):
+        for s in range(1, n):
+            for g in range(PIECES // FLIGHT):
+                if limit <= 0:
+                    return
+                if (s, g) in done or any((s, g * FLIGHT + w) not in arrived for w in range(FLIGHT)):
+                    continue
+                done.add((s, g))
+                limit -= 1
+                for k in range(2):
+                    finish(k, s, g * FLIGHT * piece, FLIGHT * piece)
+
+    while slots:
+        last = slots[0] if slots[0][0] == n - 1 and slots[0][1] >= PIECES - FLIGHT else None
+        advance(1)
+        if last:
             for k in range(2):
-                ring[s - 1, k, c].wait_recv()
-                if s < n - 1:
-                    forward(s, k, c)
-            if units:
-                finish_ahead(*units.pop(0))
-    for unit in units:
-        finish_ahead(*unit)
-    for copy in sent:
-        copy.wait_send()
+                finish(k, last[0], last[1] * piece, piece)
+            done.add((last[0], last[1] // FLIGHT))
+        if own:
+            k, start = own.pop(0)
+            own_rows(k, start, FLIGHT * piece)
+        else:
+            ready(1)
+    for k, start in own:
+        own_rows(k, start, FLIGHT * piece)
+    ready(n * PIECES)
+    with jax.named_scope("drain"):
+        for copy in sent:
+            copy.wait_send()
 
 
 def write_kernel(count, *refs):
@@ -402,25 +493,28 @@
             pltpu.VMEM((2, low_rows, columns), f32),
             pltpu.VMEM((2, low_rows, columns), f32),
             pltpu.VMEM((2, n, part, block), bf16),
-            pltpu.VMEM((2, n, block // CHUNKS, columns), bf16),
-            pltpu.VMEM((2, m, n, part, block // CHUNKS), bf16),
-            pltpu.VMEM((2, n, block // CHUNKS, rank), bf16),
+            pltpu.VMEM((2, n, block, columns), bf16),
+            pltpu.VMEM((2, m, n, part, block), bf16),
+            pltpu.VMEM((2, n, block, rank), bf16),
             pltpu.VMEM((2, m, 2, part, tokens), bf16),
             pltpu.VMEM((2, n, low_rows, columns), f32),
-            pltpu.VMEM((2, n // 2, low_rows, columns), f32),
-            pltpu.VMEM((2, n // 2, low_rows, columns), f32),
-            pltpu.VMEM((n * m, 8, 128), f32),
+            pltpu.VMEM((2, n, low_rows, columns), bf16),
+            pltpu.VMEM((2, n // 2, low_rows, columns), bf16),
+            pltpu.VMEM((2, n // 2, low_rows, columns), bf16),
+            pltpu.VMEM((2, n // 2, low_rows, columns), bf16),
+            pltpu.VMEM((2, 2, n // 2, 1, 128), f32),
+            pltpu.VMEM((n * m, 1, 128), f32),
             pltpu.VMEM((2, n, low_rows, columns), bf16),
             dma((6, 2)),
             dma((2, 2, n)),
             dma((2, 2, m)),
             dma((2, 2, n // 2)),
             dma((2, 2, n // 2)),
+            dma((2, 2, n // 2)),
             dma((2, n * m)),
             dma((2, 2, n)),
-            dma((2, 2, n - 1, CHUNKS)),
-            dma((2, 2, n)),
-            dma((2, 2, m)),
+            dma((2, 2, n - 1, PIECES)),
+            dma((2, 2, 3)),
         ],
         compiler_params=pltpu.CompilerParams(
             collective_id=0, has_side_effects=True, vmem_limit_bytes=48 * 2**20
@@ -440,9 +534,10 @@
     basis, first = args[4], args[8]
     return (
         n % 2 == 0
+        and m == 4
         and basis.shape[1] // n % 16 == 0
         and basis.shape[1] // m % 16 == 0
-        and basis.shape[0] // n % (128 * CHUNKS) == 0
+        and basis.shape[0] // n % (16 * PIECES) == 0
         and basis.shape[0] // n % 128 == 0
         and first.shape[1] // m % 128 == 0
     )

time: 138 us -> 122 us (0.88)
  Pallas kernels: 138 us -> 121 us
    pallas_call x1, Pallas kernels: 133 us -> 116 us  [fused_per_device(): pl.pallas_call(functools.partial(ring_kernel, n, m), out_shape=tuple((plt...]
where the time goes in v1:
time: 122 us
  Pallas kernels  121 us (99%)
    pallas_call x1, Pallas kernels, fused_per_device(): pl.pallas_call(functools.partial(ring_kernel, n, m), out_shape=tuple((plt...  116 us
    pallas_call x1, Pallas kernels, fused_per_device(): pl.pallas_call(functools.partial(write_kernel, len(kinds)), out_shape=tup...  4.83 us

profile of v1, /device:TPU:0, one launch (start us, length us, event | category | flops | bytes accessed | tf_op | source)
XLA Modules:
  0.0 121.9 jit_solution(7226092577761213285)
XLA Ops:
  0.6 116.3 %shard_map.195 = (f32[512,512]{1,0:T(8,128)S(1)}, f32[512,512]{1,0:T(8,128)S(1)}, f32[512,512]{1,0:T(8,128)S(1)}, f32[512,512]{1,0:T(8,128)S(1)}, f32[32,512]{1,...) custom-call(bf16[256,4096]{1,0:T(8,128)(2,1)} %refs_0_.1, ...), custom_call_target="tpu_custom_call" | custom-call | tf_op jit(solution)/shard_map/pallas_call | solution.py:483
  116.9 4.8 %shard_map.196 = (f32[512,512]{1,0:T(8,128)}, f32[512,512]{1,0:T(8,128)}, f32[512,512]{1,0:T(8,128)}, f32[512,512]{1,0:T(8,128)}, f32[32,512]{1,0:T(8,128)}, /*i...) custom-call(f32[512,512]{1,0:T(8,128)S(1)} %get-tuple-element.20.ref, ...), custom_call_target="tpu_custom_call" | custom-call | tf_op jit(solution)/shard_map/pallas_call | solution.py:523

commit v2 on v1

--- a/solution.py
+++ b/solution.py
@@ -96,10 +96,11 @@
 
 MESH = pl.DeviceIdType.MESH
 PIECES = 8
-FLIGHT = 4
-PACE = (4, 2, 2, 3, 3, 3, 3, 3, 3, 8, 6, 4)
+FLIGHT = 8
+PACE = (8, 2, 2, 3, 3, 3, 3, 3, 3, 6, 4, 4)
 STRETCH = 40.0
 REACH = 3.0
+ROWS, COORD, WIDE, UNIT, PAIR, PART, SQUARE, DIRECTION, RING = range(9)
 LN2 = 0.6931471805599453
 
 
@@ -145,7 +146,7 @@
         x_v, cot_v, basis, master_v, first, second,
         rows_v, code_v, wide_v, flat_v, coord_v, part_v, mine_v, pair_v, sum_v, got_v, unit_v,
         square_v, direction_v,
-        in_sem, rows_sem, coord_sem, pair_sem, part_sem, unit_sem, square_sem, direction_sem, ring_sem, wide_sem,
+        in_sem, out_sem, square_sem, coord_sem, rows_sem, pair_sem, part_sem, unit_sem, direction_sem, ring_sem, wide_sem,
     ) = refs[22:]
     f, t = lax.axis_index("fs"), lax.axis_index("tp")
     me = f * m + t
@@ -201,32 +202,32 @@
     with jax.named_scope("barrier"):
         pl.semaphore_wait(barrier, n * m - 1)
 
-    sent = []
-
-    def send(source, target, sems, index, device):
+    def send(source, target, out, arrival, device):
         copy = pltpu.make_async_remote_copy(
             src_ref=source,
             dst_ref=target,
-            send_sem=sems.at[(0,) + index],
-            recv_sem=sems.at[(1,) + index],
+            send_sem=out_sem.at[out],
+            recv_sem=arrival,
             device_id=device,
             device_id_type=MESH,
         )
         copy.start()
-        sent.append(copy)
         return copy
 
-    def push(own, slots, sems, k):
-        copies = {half: send(own, slots(half), sems, (k, half), {"fs": across})}
+    def wait_bytes(like, sem):
+        pltpu.make_async_copy(like, like, sem).wait()
+
+    def push(own, slots, out, sems, k):
+        copies = {half: send(own, slots(half), (out, k), sems.at[k, half], {"fs": across})}
         for d in order:
-            copies[d] = send(own, slots(d), sems, (k, d), {"fs": along(d)})
+            copies[d] = send(own, slots(d), (out, k), sems.at[k, d], {"fs": along(d)})
         return copies
 
-    def relay(copies, slots, sems, k):
+    def relay(copies, slots, out, sems, k):
         for d in order:
             with jax.named_scope(f"rows_wait#k={k}#d={d}"):
                 copies[d].wait_recv()
-            copies[half + d] = send(slots(d), slots(half + d), sems, (k, half + d), {"fs": across})
+            copies[half + d] = send(slots(d), slots(half + d), (out, k), sems.at[k, half + d], {"fs": across})
 
     place = (1 - x) * z + x * (n - 1 - z)
 
@@ -252,7 +253,7 @@
                         ring[s - 1, k, c].wait_recv()
                 if s < n - 1:
                     where = code_v.at[k, origin[s][k], pl.ds(c * piece, piece)]
-                    ring[s, k, c] = send(where, where, ring_sem, (k, s, c), {"fs": toward[k]})
+                    ring[s, k, c] = send(where, where, (RING, k), ring_sem.at[k, s, c], {"fs": toward[k]})
             if s > 0:
                 arrived.append((s, c))
 
@@ -261,7 +262,7 @@
     def rows_at(k):
         return lambda d: rows_v.at[k, d]
 
-    rows = [push(rows_v.at[k, 0], rows_at(k), rows_sem, k) for k in range(2)]
+    rows = [push(rows_v.at[k, 0], rows_at(k), ROWS, rows_sem, k) for k in range(2)]
     for i in range(PIECES // FLIGHT):
         span = pl.ds(i * FLIGHT * piece, FLIGHT * piece)
         for k in range(2):
@@ -277,9 +278,8 @@
         return lax.dot_general(left, right, (((1,), (1,)), ((), ())), preferred_element_type=jnp.float32)
 
     for k in range(2):
-        relay(rows[k], rows_at(k), rows_sem, k)
+        relay(rows[k], rows_at(k), ROWS, rows_sem, k)
         advance(pace.pop(0))
-    coords = []
     for k in range(2):
         loads["x", k].wait()
         total = coordinates(k, 0)
@@ -292,26 +292,21 @@
         high = total.astype(jnp.bfloat16)
         coord_v[k, t, 0] = high
         coord_v[k, t, 1] = (total - high.astype(jnp.float32)).astype(jnp.bfloat16)
-        coords.append(
-            [
-                send(coord_v.at[k, t], coord_v.at[k, t], coord_sem, (k, d), {"tp": lax.rem(t + d, m)})
-                for d in range(1, m)
-            ]
-        )
+        for d in range(1, m):
+            send(coord_v.at[k, t], coord_v.at[k, t], (COORD, k), coord_sem.at[k], {"tp": lax.rem(t + d, m)})
         advance(pace.pop(0))
 
     wide = []
     for k in range(2):
         for target in (opposite, partner):
-            index = (k, len(wide) % 2)
-            wide.append(send(rows_v.at[k], wide_v.at[k, t], wide_sem, index, {"tp": target}))
+            arrival = wide_sem.at[k, len(wide) % 2]
+            wide.append(send(rows_v.at[k], wide_v.at[k, t], (WIDE, k), arrival, {"tp": target}))
         wide_v[k, t] = rows_v[k]
     pairs, units = [], []
     for k in range(2):
         loads["cot", k].wait()
         with jax.named_scope(f"coords_wait#k={k}"):
-            for copy in coords[k]:
-                copy.wait_recv()
+            wait_bytes(coord_v.at[k, pl.ds(0, m - 1)], coord_sem.at[k])
         part = jnp.dot(
             coord_v[k, :, 0].reshape(rank, tokens), cot_v[k], preferred_element_type=jnp.float32
         ) + jnp.dot(coord_v[k, :, 1].reshape(rank, tokens), cot_v[k], preferred_element_type=jnp.float32)
@@ -320,10 +315,12 @@
         mine_v[k] = code.reshape(n, low_rows, columns)
         unit_v[0, k, 0] = jnp.broadcast_to(unit, unit_v.shape[3:])
         pairs.append({})
-        units.append({0: send(unit_v.at[0, k, 0], unit_v.at[1, k, 0], unit_sem, (k, 0), {"fs": across})})
+        units.append(
+            {0: send(unit_v.at[0, k, 0], unit_v.at[1, k, 0], (UNIT, k), unit_sem.at[k, 0], {"fs": across})}
+        )
         for d in (*order, 0):
             pairs[k][d] = send(
-                mine_v.at[k, along(d, 1 - x)], pair_v.at[k, d], pair_sem, (k, d), {"fs": across}
+                mine_v.at[k, along(d, 1 - x)], pair_v.at[k, d], (PAIR, k), pair_sem.at[k, d], {"fs": across}
             )
         advance(pace.pop(0))
     parts = []
@@ -339,8 +336,9 @@
             code, unit = encode_scaled(paired(k, d))
             sum_v[k, d] = code
             unit_v[0, k, d] = jnp.broadcast_to(unit, unit_v.shape[3:])
-            units[k][d] = send(unit_v.at[0, k, d], unit_v.at[1, k, d], unit_sem, (k, d), {"fs": along(d)})
-            parts[k][d] = send(sum_v.at[k, d], got_v.at[k, d], part_sem, (k, d), {"fs": along(d)})
+            there = {"fs": along(d)}
+            units[k][d] = send(unit_v.at[0, k, d], unit_v.at[1, k, d], (UNIT, k), unit_sem.at[k, d], there)
+            parts[k][d] = send(sum_v.at[k, d], got_v.at[k, d], (PART, k), part_sem.at[k, d], there)
         advance(pace.pop(0))
 
     lows = []
@@ -355,19 +353,16 @@
         lows.append(low)
         squares = squares + jnp.sum(low * low)
     square_v[0] = jnp.full(square_v.shape[1:], squares, jnp.float32)
-    copies = []
     for d in range(1, n * m):
         other = lax.rem(me + d, n * m)
-        copies.append(
-            send(square_v.at[0], square_v.at[d], square_sem, (d,), {"fs": other // m, "tp": lax.rem(other, m)})
-        )
+        there = {"fs": other // m, "tp": lax.rem(other, m)}
+        send(square_v.at[0], square_v.at[d], (SQUARE, 0), square_sem, there)
     advance(pace.pop(0))
     for k in range(2):
         loads["first", k].wait()
         loads["second", k].wait()
     with jax.named_scope("square_wait"):
-        for copy in copies:
-            copy.wait_recv()
+        wait_bytes(square_v.at[pl.ds(1, n * m - 1)], square_sem)
     total_squares = jnp.sum(square_v[...], axis=0)[:1, :1]
     factor = 1.0 / jnp.sqrt(1.0 + total_squares / (2.0 * rank * (columns * m)))
 
@@ -376,20 +371,21 @@
         new_first, new_second, direction = moment_update(lows[k], factor, first[k], second[k])
         direction_v[k, f] = direction
         own = direction_v.at[k, f]
-        directions.append(push(own, lambda d: own, direction_sem, k))
+        directions.append(push(own, lambda d: own, DIRECTION, direction_sem, k))
         first_out[k][...] = new_first
         second_out[k][...] = new_second
     advance(pace.pop(0))
     for k in range(2):
         wide[2 * k].wait_recv()
         there = wide_v.at[k, opposite]
-        wide.append(send(there, there, wide_sem, (k, 2), {"tp": partner}))
+        wide.append(send(there, there, (WIDE, k), wide_sem.at[k, 2], {"tp": partner}))
     for k in range(2):
         for d in order:
             with jax.named_scope(f"direction_wait#k={k}#d={d}"):
                 directions[k][d].wait_recv()
             there = direction_v.at[k, along(-d)]
-            directions[k][half + d] = send(there, there, direction_sem, (k, half + d), {"fs": across})
+            arrival = direction_sem.at[k, half + d]
+            directions[k][half + d] = send(there, there, (DIRECTION, k), arrival, {"fs": across})
     advance(pace.pop(0))
     with jax.named_scope("wide_wait"):
         for copy in (wide[1], wide[3], wide[4], wide[5]):
@@ -454,8 +450,16 @@
         own_rows(k, start, FLIGHT * piece)
     ready(n * PIECES)
     with jax.named_scope("drain"):
-        for copy in sent:
-            copy.wait_send()
+        for k in range(2):
+            wait_bytes(code_v.at[k, pl.ds(0, n - 1)], out_sem.at[RING, k])
+            wait_bytes(rows_v.at[k, pl.ds(0, n - 1)], out_sem.at[ROWS, k])
+            wait_bytes(coord_v.at[k, pl.ds(0, m - 1)], out_sem.at[COORD, k])
+            wait_bytes(wide_v.at[k, pl.ds(0, m - 1)], out_sem.at[WIDE, k])
+            wait_bytes(unit_v.at[0, k], out_sem.at[UNIT, k])
+            wait_bytes(pair_v.at[k], out_sem.at[PAIR, k])
+            wait_bytes(got_v.at[k, pl.ds(1, half - 1)], out_sem.at[PART, k])
+            wait_bytes(direction_v.at[k, pl.ds(0, n - 1)], out_sem.at[DIRECTION, k])
+        wait_bytes(square_v.at[pl.ds(1, n * m - 1)], out_sem.at[SQUARE, 0])
 
 
 def write_kernel(count, *refs):
@@ -506,15 +510,16 @@
             pltpu.VMEM((n * m, 1, 128), f32),
             pltpu.VMEM((2, n, low_rows, columns), bf16),
             dma((6, 2)),
-            dma((2, 2, n)),
-            dma((2, 2, m)),
-            dma((2, 2, n // 2)),
-            dma((2, 2, n // 2)),
-            dma((2, 2, n // 2)),
-            dma((2, n * m)),
-            dma((2, 2, n)),
-            dma((2, 2, n - 1, PIECES)),
-            dma((2, 2, 3)),
+            dma((9, 2)),
+            dma,
+            dma((2,)),
+            dma((2, n)),
+            dma((2, n // 2)),
+            dma((2, n // 2)),
+            dma((2, n // 2)),
+            dma((2, n)),
+            dma((2, n - 1, PIECES)),
+            dma((2, 3)),
         ],
         compiler_params=pltpu.CompilerParams(
             collective_id=0, has_side_effects=True, vmem_limit_bytes=48 * 2**20

time: 122 us -> 118 us (0.967)
  Pallas kernels: 121 us -> 117 us
    pallas_call x1, Pallas kernels: 116 us -> 112 us  [fused_per_device(): pl.pallas_call(functools.partial(ring_kernel, n, m), out_shape=tuple((plt...]
where the time goes in v2:
time: 118 us
  Pallas kernels  117 us (99%)
    pallas_call x1, Pallas kernels, fused_per_device(): pl.pallas_call(functools.partial(ring_kernel, n, m), out_shape=tuple((plt...  112 us
    pallas_call x1, Pallas kernels, fused_per_device(): pl.pallas_call(functools.partial(write_kernel, len(kinds)), out_shape=tup...  4.83 us

profile of v2, /device:TPU:0, one launch (start us, length us, event | category | flops | bytes accessed | tf_op | source)
XLA Modules:
  0.0 117.8 jit_solution(3152466673260228602)
XLA Ops:
  0.6 112.1 %shard_map.195 = (f32[512,512]{1,0:T(8,128)S(1)}, f32[512,512]{1,0:T(8,128)S(1)}, f32[512,512]{1,0:T(8,128)S(1)}, f32[512,512]{1,0:T(8,128)S(1)}, f32[32,512]{1,...) custom-call(bf16[256,4096]{1,0:T(8,128)(2,1)} %refs_0_.1, ...), custom_call_target="tpu_custom_call" | custom-call | tf_op jit(solution)/shard_map/pallas_call | solution.py:487
  112.8 4.8 %shard_map.196 = (f32[512,512]{1,0:T(8,128)}, f32[512,512]{1,0:T(8,128)}, f32[512,512]{1,0:T(8,128)}, f32[512,512]{1,0:T(8,128)}, f32[32,512]{1,0:T(8,128)}, /*i...) custom-call(f32[512,512]{1,0:T(8,128)S(1)} %get-tuple-element.20.ref, ...), custom_call_target="tpu_custom_call" | custom-call | tf_op jit(solution)/shard_map/pallas_call | solution.py:528

commit v3 on v2

--- a/solution.py
+++ b/solution.py
@@ -97,10 +97,11 @@
 MESH = pl.DeviceIdType.MESH
 PIECES = 8
 FLIGHT = 8
-PACE = (8, 2, 2, 3, 3, 3, 3, 3, 3, 6, 4, 4)
+PACE = (4, 2, 2, 4, 1, 2, 3, 5, 3, 4, 4, 6, 4, 4)
 STRETCH = 40.0
 REACH = 3.0
-ROWS, COORD, WIDE, UNIT, PAIR, PART, SQUARE, DIRECTION, RING = range(9)
+SPLITS = 8
+ROWS, COORD, WIDE, UNIT, PAIR, CROSS, SQUARE, DIRECTION, RING = range(9)
 LN2 = 0.6931471805599453
 
 
@@ -115,8 +116,8 @@
 def decode(code):
     code = code.astype(jnp.float32)
     size = jnp.abs(code)
-    near = size * (1.0 - size * (0.5 - size * (1.0 / 3.0)))
-    value = jnp.where(size < 0.02, near, jnp.log(1.0 + size)) * (1.0 / (LN2 * STRETCH))
+    unit = 1.0 / (LN2 * STRETCH)
+    value = jnp.where(size < 0.004, size * (unit - size * (0.5 * unit)), jnp.log(1.0 + size) * unit)
     return jnp.where(code < 0.0, -value, value)
 
 
@@ -144,9 +145,9 @@
     )
     (
         x_v, cot_v, basis, master_v, first, second,
-        rows_v, code_v, wide_v, flat_v, coord_v, part_v, mine_v, pair_v, sum_v, got_v, unit_v,
+        rows_v, code_v, plain_v, wide_v, flat_v, coord_v, part_v, mine_v, sum_v, got_v, both_v, cross_v, unit_v,
         square_v, direction_v,
-        in_sem, out_sem, square_sem, coord_sem, rows_sem, pair_sem, part_sem, unit_sem, direction_sem, ring_sem, wide_sem,
+        in_sem, out_sem, square_sem, coord_sem, rows_sem, got_sem, cross_sem, unit_sem, direction_sem, ring_sem, wide_sem,
     ) = refs[22:]
     f, t = lax.axis_index("fs"), lax.axis_index("tp")
     me = f * m + t
@@ -160,14 +161,17 @@
     z, x = f // 2, lax.rem(f, 2)
     across = z * 2 + 1 - x
     partner, opposite = t + 1 - 2 * lax.rem(t, 2), lax.rem(t + m // 2, m)
-    order = (1, half - 1, *range(2, half - 1))
-
-    def along(d, side=None):
-        side = x if side is None else side
-        return lax.rem(z + d + half, half) * 2 + side
-
-    def source_of(d):
-        return along(-(d % half), x if d < half else 1 - x)
+    even = lax.rem(z, 2) == 0
+    inner = (z > 0) & (z < half - 1)
+    outer = jnp.logical_not(inner)
+    low_side = z < half // 2
+    far, near = jnp.where(low_side, 3, 0), jnp.where(low_side, 2, 1)
+    mate = jnp.where(even, z + 1, z - 1)
+    reach = (jnp.where(even, 1, 2), jnp.where(low_side, jnp.where(even, 2, 0), jnp.where(even, 3, 1)))
+    heard = (*reach, far)
+
+    def column(to):
+        return {"fs": to * 2 + x}
 
     loads = {}
     for i, (name, sources, target) in enumerate(
@@ -196,7 +200,7 @@
     select = jnp.where(chosen, 1.0, 0.0).astype(jnp.bfloat16)
     for k in range(2):
         loads["basis", k].wait()
-        rows_v[k, 0] = lax.dot_general(
+        rows_v[k, f] = lax.dot_general(
             select, basis[k], (((1,), (1,)), ((), ())), preferred_element_type=jnp.float32
         ).astype(jnp.bfloat16)
     with jax.named_scope("barrier"):
@@ -217,17 +221,34 @@
     def wait_bytes(like, sem):
         pltpu.make_async_copy(like, like, sem).wait()
 
-    def push(own, slots, out, sems, k):
-        copies = {half: send(own, slots(half), (out, k), sems.at[k, half], {"fs": across})}
-        for d in order:
-            copies[d] = send(own, slots(d), (out, k), sems.at[k, d], {"fs": along(d)})
-        return copies
-
-    def relay(copies, slots, out, sems, k):
-        for d in order:
-            with jax.named_scope(f"rows_wait#k={k}#d={d}"):
-                copies[d].wait_recv()
-            copies[half + d] = send(slots(d), slots(half + d), (out, k), sems.at[k, half + d], {"fs": across})
+    def push(block_at, out, sems, k):
+        own = block_at(f)
+        send(own, own, (out, k), sems.at[k, f], {"fs": across})
+        for to in reach:
+            send(own, own, (out, k), sems.at[k, f], column(to))
+
+    def arrive(like, sem):
+        pltpu.make_async_copy(like, like, sem).wait()
+
+    def relay(block_at, out, sems, k):
+        for i, of in enumerate(heard):
+            origin_of = of * 2 + x
+            there = block_at(origin_of)
+            with jax.named_scope(f"relay_wait#o={out}#k={k}#i={i}"):
+                arrive(there, sems.at[k, origin_of])
+            if i != 1:
+
+                @pl.when(inner)
+                def _():
+                    send(there, there, (out, k), sems.at[k, origin_of], column(mate))
+
+            send(there, there, (out, k), sems.at[k, origin_of], {"fs": across})
+
+    def late(block_at, out, sems, k):
+        for i, of in enumerate((z, *heard)):
+            origin_of = of * 2 + 1 - x
+            with jax.named_scope(f"late_wait#o={out}#k={k}#i={i}"):
+                arrive(block_at(origin_of), sems.at[k, origin_of])
 
     place = (1 - x) * z + x * (n - 1 - z)
 
@@ -242,9 +263,9 @@
     slots = [
         (s, g * FLIGHT + w) for g in range(PIECES // FLIGHT) for s in range(n) for w in range(FLIGHT)
     ]
-    arrived = []
-
-    def advance(count):
+    arrived, fresh = [], []
+
+    def advance(count, relaxed=True):
         for _ in range(min(count, len(slots))):
             s, c = slots.pop(0)
             for k in range(2):
@@ -256,13 +277,24 @@
                     ring[s, k, c] = send(where, where, (RING, k), ring_sem.at[k, s, c], {"fs": toward[k]})
             if s > 0:
                 arrived.append((s, c))
+                fresh.append((s, c))
+        if relaxed:
+            unfold()
+
+    def unfold():
+        for s, c in fresh:
+            span = pl.ds(c * piece, piece)
+            for k in range(2):
+                plain_v[k, origin[s][k], span] = decode(code_v[k, origin[s][k], span])
+        fresh.clear()
 
     pace = list(PACE)
 
     def rows_at(k):
-        return lambda d: rows_v.at[k, d]
-
-    rows = [push(rows_v.at[k, 0], rows_at(k), ROWS, rows_sem, k) for k in range(2)]
+        return lambda of: rows_v.at[k, of]
+
+    for k in range(2):
+        push(rows_at(k), ROWS, rows_sem, k)
     for i in range(PIECES // FLIGHT):
         span = pl.ds(i * FLIGHT * piece, FLIGHT * piece)
         for k in range(2):
@@ -272,23 +304,22 @@
         if i == 0:
             advance(pace.pop(0))
 
-    def coordinates(k, d):
-        left = rows_v[k, d]
-        right = x_v[k, :, pl.ds(pl.multiple_of(source_of(d) * block, block), block)]
+    def coordinates(k, of):
+        left = rows_v[k, of]
+        right = x_v[k, :, pl.ds(pl.multiple_of(of * block, block), block)]
         return lax.dot_general(left, right, (((1,), (1,)), ((), ())), preferred_element_type=jnp.float32)
 
     for k in range(2):
-        relay(rows[k], rows_at(k), ROWS, rows_sem, k)
+        relay(rows_at(k), ROWS, rows_sem, k)
         advance(pace.pop(0))
     for k in range(2):
         loads["x", k].wait()
-        total = coordinates(k, 0)
-        for d in range(1, half):
-            total = total + coordinates(k, d)
-        for d in range(half, n):
-            with jax.named_scope(f"rows_late#k={k}#d={d}"):
-                rows[k][d].wait_recv()
-            total = total + coordinates(k, d)
+        total = coordinates(k, f)
+        for of in heard:
+            total = total + coordinates(k, of * 2 + x)
+        late(rows_at(k), ROWS, rows_sem, k)
+        for of in (z, *heard):
+            total = total + coordinates(k, of * 2 + 1 - x)
         high = total.astype(jnp.bfloat16)
         coord_v[k, t, 0] = high
         coord_v[k, t, 1] = (total - high.astype(jnp.float32)).astype(jnp.bfloat16)
@@ -302,7 +333,19 @@
             arrival = wide_sem.at[k, len(wide) % 2]
             wide.append(send(rows_v.at[k], wide_v.at[k, t], (WIDE, k), arrival, {"tp": target}))
         wide_v[k, t] = rows_v[k]
-    pairs, units = [], []
+    pair_rows = 2 * low_rows
+
+    def ship(k, source, unit, slot, device):
+        unit_out, unit_in = unit_v.at[0, k, unit], unit_v.at[1, k, slot]
+        send(unit_out, unit_in, (UNIT, k), unit_sem.at[k, slot], device)
+        send(source, got_v.at[k, slot], (PAIR, k), got_sem.at[k, slot], device)
+
+    def taken(k, slot):
+        with jax.named_scope(f"got_wait#k={k}#slot={slot}"):
+            arrive(unit_v.at[1, k, slot], unit_sem.at[k, slot])
+            arrive(got_v.at[k, slot], got_sem.at[k, slot])
+        return decode(got_v[k, slot]) * unit_v[1, k, slot][:1, :1]
+
     for k in range(2):
         loads["cot", k].wait()
         with jax.named_scope(f"coords_wait#k={k}"):
@@ -310,46 +353,51 @@
         part = jnp.dot(
             coord_v[k, :, 0].reshape(rank, tokens), cot_v[k], preferred_element_type=jnp.float32
         ) + jnp.dot(coord_v[k, :, 1].reshape(rank, tokens), cot_v[k], preferred_element_type=jnp.float32)
-        part_v[k] = part.reshape(n, low_rows, columns)
+        part_v[k] = part.reshape(half, pair_rows, columns)
         code, unit = encode_scaled(part)
-        mine_v[k] = code.reshape(n, low_rows, columns)
+        mine_v[k] = code.reshape(half, pair_rows, columns)
         unit_v[0, k, 0] = jnp.broadcast_to(unit, unit_v.shape[3:])
-        pairs.append({})
-        units.append(
-            {0: send(unit_v.at[0, k, 0], unit_v.at[1, k, 0], (UNIT, k), unit_sem.at[k, 0], {"fs": across})}
-        )
-        for d in (*order, 0):
-            pairs[k][d] = send(
-                mine_v.at[k, along(d, 1 - x)], pair_v.at[k, d], (PAIR, k), pair_sem.at[k, d], {"fs": across}
-            )
+
+        @pl.when(outer)
+        def _():
+            ship(k, mine_v.at[k, far], 0, 0, column(mate))
+            ship(k, mine_v.at[k, near], 0, 1, column(mate))
+
+        ship(k, mine_v.at[k, mate], 0, 2, column(mate))
         advance(pace.pop(0))
-    parts = []
-    def paired(k, d):
-        with jax.named_scope(f"pair_wait#k={k}#d={d}"):
-            pairs[k][d].wait_recv()
-        return decode(pair_v[k, d]) * unit_v[1, k, 0][:1, :1] + part_v[k, along(d)]
-
-    for k in range(2):
-        parts.append({})
-        units[k][0].wait_recv()
-        for d in order:
-            code, unit = encode_scaled(paired(k, d))
-            sum_v[k, d] = code
-            unit_v[0, k, d] = jnp.broadcast_to(unit, unit_v.shape[3:])
-            there = {"fs": along(d)}
-            units[k][d] = send(unit_v.at[0, k, d], unit_v.at[1, k, d], (UNIT, k), unit_sem.at[k, d], there)
-            parts[k][d] = send(sum_v.at[k, d], got_v.at[k, d], (PART, k), part_sem.at[k, d], there)
+    for k in range(2):
+
+        @pl.when(inner)
+        def _():
+            for slot, to in enumerate((far, near)):
+                code, unit = encode_scaled(taken(k, slot) + part_v[k, to])
+                sum_v[k, slot] = code
+                unit_v[0, k, 1 + slot] = jnp.broadcast_to(unit, unit_v.shape[3:])
+                ship(k, sum_v.at[k, slot], 1 + slot, 3, column(to))
+
         advance(pace.pop(0))
-
+    for k in range(2):
+        both = part_v[k, z] + taken(k, 2) + taken(k, 3)
+        both_v[k] = both.reshape(2, low_rows, columns)
+        code, unit = encode_scaled(both_v[k, 1 - x])
+        cross_v[k, 0] = code
+        unit_v[0, k, 3] = jnp.broadcast_to(unit, unit_v.shape[3:])
+        there = {"fs": across}
+        send(unit_v.at[0, k, 3], unit_v.at[1, k, 4], (UNIT, k), unit_sem.at[k, 4], there)
+        send(cross_v.at[k, 0], cross_v.at[k, 1], (CROSS, k), cross_sem.at[k], there)
+        advance(pace.pop(0))
+
+    for k in range(2):
+        wide[2 * k].wait_recv()
+        there = wide_v.at[k, opposite]
+        wide.append(send(there, there, (WIDE, k), wide_sem.at[k, 2], {"tp": partner}))
     lows = []
     squares = jnp.zeros((), jnp.float32)
     for k in range(2):
-        low = paired(k, 0)
-        for d in range(1, half):
-            with jax.named_scope(f"part_wait#k={k}#d={d}"):
-                units[k][d].wait_recv()
-                parts[k][d].wait_recv()
-            low = low + decode(got_v[k, d]) * unit_v[1, k, d][:1, :1]
+        with jax.named_scope(f"cross_wait#k={k}"):
+            arrive(unit_v.at[1, k, 4], unit_sem.at[k, 4])
+            arrive(cross_v.at[k, 1], cross_sem.at[k])
+        low = both_v[k, x] + decode(cross_v[k, 1]) * unit_v[1, k, 4][:1, :1]
         lows.append(low)
         squares = squares + jnp.sum(low * low)
     square_v[0] = jnp.full(square_v.shape[1:], squares, jnp.float32)
@@ -358,6 +406,13 @@
         there = {"fs": other // m, "tp": lax.rem(other, m)}
         send(square_v.at[0], square_v.at[d], (SQUARE, 0), square_sem, there)
     advance(pace.pop(0))
+    with jax.named_scope("wide_wait"):
+        for copy in (wide[1], wide[3], wide[4], wide[5]):
+            copy.wait_recv()
+    for k in range(2):
+        for d in range(1, n):
+            of = lax.rem(f + d, n)
+            flat_v[k, of] = wide_v[k, :, of].reshape(rank, block).T
     for k in range(2):
         loads["first", k].wait()
         loads["second", k].wait()
@@ -366,37 +421,21 @@
     total_squares = jnp.sum(square_v[...], axis=0)[:1, :1]
     factor = 1.0 / jnp.sqrt(1.0 + total_squares / (2.0 * rank * (columns * m)))
 
-    directions = []
+    def directions_at(k):
+        return lambda of: direction_v.at[k, of]
+
     for k in range(2):
         new_first, new_second, direction = moment_update(lows[k], factor, first[k], second[k])
         direction_v[k, f] = direction
-        own = direction_v.at[k, f]
-        directions.append(push(own, lambda d: own, DIRECTION, direction_sem, k))
+        push(directions_at(k), DIRECTION, direction_sem, k)
         first_out[k][...] = new_first
         second_out[k][...] = new_second
     advance(pace.pop(0))
     for k in range(2):
-        wide[2 * k].wait_recv()
-        there = wide_v.at[k, opposite]
-        wide.append(send(there, there, (WIDE, k), wide_sem.at[k, 2], {"tp": partner}))
-    for k in range(2):
-        for d in order:
-            with jax.named_scope(f"direction_wait#k={k}#d={d}"):
-                directions[k][d].wait_recv()
-            there = direction_v.at[k, along(-d)]
-            arrival = direction_sem.at[k, half + d]
-            directions[k][half + d] = send(there, there, (DIRECTION, k), arrival, {"fs": across})
+        relay(directions_at(k), DIRECTION, direction_sem, k)
     advance(pace.pop(0))
-    with jax.named_scope("wide_wait"):
-        for copy in (wide[1], wide[3], wide[4], wide[5]):
-            copy.wait_recv()
-    for k in range(2):
-        for d in range(1, n):
-            flat_v[k, source_of(d)] = wide_v[k, :, d].reshape(rank, block).T
-    for k in range(2):
-        for d in range(half, n):
-            with jax.named_scope(f"direction_late#k={k}#d={d}"):
-                directions[k][d].wait_recv()
+    for k in range(2):
+        late(directions_at(k), DIRECTION, direction_sem, k)
 
     def own_rows(k, start, size):
         span = pl.ds(start, size)
@@ -416,7 +455,7 @@
             direction_v[k].reshape(rank, columns),
             preferred_element_type=jnp.float32,
         )
-        weight = decode(code_v[k, source, span]) - rate * step
+        weight = plain_v[k, source, span] - rate * step
         gathered[k][pl.ds(pl.multiple_of(source * block + start, size), size)] = weight.astype(jnp.bfloat16)
 
     own = [(k, i * FLIGHT * piece) for i in range(PIECES // FLIGHT) for k in range(2)]
@@ -452,23 +491,36 @@
     with jax.named_scope("drain"):
         for k in range(2):
             wait_bytes(code_v.at[k, pl.ds(0, n - 1)], out_sem.at[RING, k])
-            wait_bytes(rows_v.at[k, pl.ds(0, n - 1)], out_sem.at[ROWS, k])
+            for ref, out in ((rows_v, ROWS), (direction_v, DIRECTION)):
+
+                @pl.when(inner)
+                def _():
+                    wait_bytes(ref.at[k, pl.ds(0, 8)], out_sem.at[out, k])
+
+                @pl.when(outer)
+                def _():
+                    wait_bytes(ref.at[k, pl.ds(0, 6)], out_sem.at[out, k])
+
             wait_bytes(coord_v.at[k, pl.ds(0, m - 1)], out_sem.at[COORD, k])
             wait_bytes(wide_v.at[k, pl.ds(0, m - 1)], out_sem.at[WIDE, k])
-            wait_bytes(unit_v.at[0, k], out_sem.at[UNIT, k])
-            wait_bytes(pair_v.at[k], out_sem.at[PAIR, k])
-            wait_bytes(got_v.at[k, pl.ds(1, half - 1)], out_sem.at[PART, k])
-            wait_bytes(direction_v.at[k, pl.ds(0, n - 1)], out_sem.at[DIRECTION, k])
+            wait_bytes(unit_v.at[0, k, pl.ds(0, 4)], out_sem.at[UNIT, k])
+            wait_bytes(got_v.at[k, pl.ds(0, 3)], out_sem.at[PAIR, k])
+            wait_bytes(cross_v.at[k, 0], out_sem.at[CROSS, k])
         wait_bytes(square_v.at[pl.ds(1, n * m - 1)], out_sem.at[SQUARE, 0])
 
 
 def write_kernel(count, *refs):
     sem = refs[2 * count]
-    copies = [pltpu.make_async_copy(refs[i], refs[count + i], sem.at[i]) for i in range(count)]
-    for copy in copies:
-        copy.start()
-    for copy in copies:
-        copy.wait()
+    copies = []
+    for i in reversed(range(count)):
+        rows = refs[i].shape[0]
+        span = rows // SPLITS if rows % (SPLITS * 16) == 0 else rows
+        for start in range(0, rows, span):
+            part = pl.ds(start, span)
+            copies.append(pltpu.make_async_copy(refs[i].at[part], refs[count + i].at[part], sem.at[i]))
+            copies[-1].start()
+    for i in range(count):
+        pltpu.make_async_copy(refs[i], refs[count + i], sem.at[i]).wait()
 
 
 def fused_per_device(n, m, *args):
@@ -498,15 +550,17 @@
             pltpu.VMEM((2, low_rows, columns), f32),
             pltpu.VMEM((2, n, part, block), bf16),
             pltpu.VMEM((2, n, block, columns), bf16),
+            pltpu.VMEM((2, n, block, columns), f32),
             pltpu.VMEM((2, m, n, part, block), bf16),
             pltpu.VMEM((2, n, block, rank), bf16),
             pltpu.VMEM((2, m, 2, part, tokens), bf16),
-            pltpu.VMEM((2, n, low_rows, columns), f32),
-            pltpu.VMEM((2, n, low_rows, columns), bf16),
-            pltpu.VMEM((2, n // 2, low_rows, columns), bf16),
-            pltpu.VMEM((2, n // 2, low_rows, columns), bf16),
-            pltpu.VMEM((2, n // 2, low_rows, columns), bf16),
-            pltpu.VMEM((2, 2, n // 2, 1, 128), f32),
+            pltpu.VMEM((2, n // 2, 2 * low_rows, columns), f32),
+            pltpu.VMEM((2, n // 2, 2 * low_rows, columns), bf16),
+            pltpu.VMEM((2, 2, 2 * low_rows, columns), bf16),
+            pltpu.VMEM((2, 4, 2 * low_rows, columns), bf16),
+            pltpu.VMEM((2, 2, low_rows, columns), f32),
+            pltpu.VMEM((2, 2, low_rows, columns), bf16),
+            pltpu.VMEM((2, 2, 5, 1, 128), f32),
             pltpu.VMEM((n * m, 1, 128), f32),
             pltpu.VMEM((2, n, low_rows, columns), bf16),
             dma((6, 2)),
@@ -514,15 +568,15 @@
             dma,
             dma((2,)),
             dma((2, n)),
-            dma((2, n // 2)),
-            dma((2, n // 2)),
-            dma((2, n // 2)),
+            dma((2, 4)),
+            dma((2,)),
+            dma((2, 5)),
             dma((2, n)),
             dma((2, n - 1, PIECES)),
             dma((2, 3)),
         ],
         compiler_params=pltpu.CompilerParams(
-            collective_id=0, has_side_effects=True, vmem_limit_bytes=48 * 2**20
+            collective_id=0, has_side_effects=True, vmem_limit_bytes=50 * 2**20
         ),
     )(*args)
     return pl.pallas_call(
@@ -538,7 +592,7 @@
 def fits(n, m, *args):
     basis, first = args[4], args[8]
     return (
-        n % 2 == 0
+        n == 8
         and m == 4
         and basis.shape[1] // n % 16 == 0
         and basis.shape[1] // m % 16 == 0

time: 118 us -> 116 us (0.983)
  Pallas kernels: 117 us -> 115 us
    pallas_call x1, Pallas kernels: 112 us -> 111 us  [fused_per_device(): pl.pallas_call(functools.partial(ring_kernel, n, m), out_shape=tuple((plt...]
where the time goes in v3:
time: 116 us
  Pallas kernels  115 us (99%)
    pallas_call x1, Pallas kernels, fused_per_device(): pl.pallas_call(functools.partial(ring_kernel, n, m), out_shape=tuple((plt...  111 us
    pallas_call x1, Pallas kernels, fused_per_device(): pl.pallas_call(functools.partial(write_kernel, len(kinds)), out_shape=tup...  4.69 us

profile of v3, /device:TPU:0, one launch (start us, length us, event | category | flops | bytes accessed | tf_op | source)
XLA Modules:
  0.0 116.3 jit_solution(9303211767358092002)
XLA Ops:
  0.6 110.8 %shard_map.195 = (f32[512,512]{1,0:T(8,128)S(1)}, f32[512,512]{1,0:T(8,128)S(1)}, f32[512,512]{1,0:T(8,128)S(1)}, f32[512,512]{1,0:T(8,128)S(1)}, f32[32,512]{1,...) custom-call(bf16[256,4096]{1,0:T(8,128)(2,1)} %refs_0_.1, ...), custom_call_target="tpu_custom_call" | custom-call | tf_op jit(solution)/shard_map/pallas_call | solution.py:539
  111.4 4.7 %shard_map.196 = (f32[512,512]{1,0:T(8,128)}, f32[512,512]{1,0:T(8,128)}, f32[512,512]{1,0:T(8,128)}, f32[512,512]{1,0:T(8,128)}, f32[32,512]{1,0:T(8,128)}, /*i...) custom-call(f32[512,512]{1,0:T(8,128)S(1)} %get-tuple-element.20.ref, ...), custom_call_target="tpu_custom_call" | custom-call | tf_op jit(solution)/shard_map/pallas_call | solution.py:582

commit v4 on v3

--- a/solution.py
+++ b/solution.py
@@ -97,11 +97,12 @@
 MESH = pl.DeviceIdType.MESH
 PIECES = 8
 FLIGHT = 8
-PACE = (4, 2, 2, 4, 1, 2, 3, 5, 3, 4, 4, 6, 4, 4)
+PACE = (3, 2, 2, 4, 2, 3, 2, 5, 3, 4, 4, 7, 4, 4)
 STRETCH = 40.0
 REACH = 3.0
 SPLITS = 8
-ROWS, COORD, WIDE, UNIT, PAIR, CROSS, SQUARE, DIRECTION, RING = range(9)
+ROWS, COORD, WIDE, UNIT, PAIR, CROSS, SQUARE, DIRECTION, RING, SHIFT = range(10)
+SHIFTED = ((DIRECTION, 0), (DIRECTION, 1))
 LN2 = 0.6931471805599453
 
 
@@ -206,8 +207,8 @@
     with jax.named_scope("barrier"):
         pl.semaphore_wait(barrier, n * m - 1)
 
-    def send(source, target, out, arrival, device):
-        copy = pltpu.make_async_remote_copy(
+    def describe(source, target, out, arrival, device):
+        return pltpu.make_async_remote_copy(
             src_ref=source,
             dst_ref=target,
             send_sem=out_sem.at[out],
@@ -215,6 +216,9 @@
             device_id=device,
             device_id_type=MESH,
         )
+
+    def send(*args):
+        copy = describe(*args)
         copy.start()
         return copy
 
@@ -242,13 +246,21 @@
                 def _():
                     send(there, there, (out, k), sems.at[k, origin_of], column(mate))
 
-            send(there, there, (out, k), sems.at[k, origin_of], {"fs": across})
+            relayed = describe(there, there, (out, k), sems.at[k, origin_of], {"fs": across})
+            if i == 2 and (out, k) in SHIFTED:
+                pl.when(inner)(relayed.start)
+            else:
+                relayed.start()
 
     def late(block_at, out, sems, k):
-        for i, of in enumerate((z, *heard)):
+        for i, of in enumerate((far, z, *reach)):
             origin_of = of * 2 + 1 - x
+            there = block_at(origin_of)
             with jax.named_scope(f"late_wait#o={out}#k={k}#i={i}"):
-                arrive(block_at(origin_of), sems.at[k, origin_of])
+                arrive(there, sems.at[k, origin_of])
+            if i == 0 and (out, k) in SHIFTED:
+                onward = describe(there, there, (SHIFT + (out == ROWS), k), sems.at[k, origin_of], column(mate))
+                pl.when(inner)(onward.start)
 
     place = (1 - x) * z + x * (n - 1 - z)
 
@@ -363,7 +375,8 @@
             ship(k, mine_v.at[k, far], 0, 0, column(mate))
             ship(k, mine_v.at[k, near], 0, 1, column(mate))
 
-        ship(k, mine_v.at[k, mate], 0, 2, column(mate))
+            ship(k, mine_v.at[k, mate], 0, 2, column(mate))
+
         advance(pace.pop(0))
     for k in range(2):
 
@@ -373,17 +386,26 @@
                 code, unit = encode_scaled(taken(k, slot) + part_v[k, to])
                 sum_v[k, slot] = code
                 unit_v[0, k, 1 + slot] = jnp.broadcast_to(unit, unit_v.shape[3:])
-                ship(k, sum_v.at[k, slot], 1 + slot, 3, column(to))
+                ship(k, sum_v.at[k, slot], 1 + slot, 4 - slot, column(near))
 
         advance(pace.pop(0))
     for k in range(2):
-        both = part_v[k, z] + taken(k, 2) + taken(k, 3)
+
+        @pl.when(inner)
+        def _():
+            code, unit = encode_scaled(taken(k, 4) + part_v[k, mate])
+            sum_v[k, 2] = code
+            unit_v[0, k, 4] = jnp.broadcast_to(unit, unit_v.shape[3:])
+            ship(k, sum_v.at[k, 2], 4, 2, column(mate))
+            part_v[k, z] = part_v[k, z] + taken(k, 3)
+
+        both = part_v[k, z] + taken(k, 2)
         both_v[k] = both.reshape(2, low_rows, columns)
         code, unit = encode_scaled(both_v[k, 1 - x])
         cross_v[k, 0] = code
         unit_v[0, k, 3] = jnp.broadcast_to(unit, unit_v.shape[3:])
         there = {"fs": across}
-        send(unit_v.at[0, k, 3], unit_v.at[1, k, 4], (UNIT, k), unit_sem.at[k, 4], there)
+        send(unit_v.at[0, k, 3], unit_v.at[1, k, 5], (UNIT, k), unit_sem.at[k, 5], there)
         send(cross_v.at[k, 0], cross_v.at[k, 1], (CROSS, k), cross_sem.at[k], there)
         advance(pace.pop(0))
 
@@ -395,9 +417,9 @@
     squares = jnp.zeros((), jnp.float32)
     for k in range(2):
         with jax.named_scope(f"cross_wait#k={k}"):
-            arrive(unit_v.at[1, k, 4], unit_sem.at[k, 4])
+            arrive(unit_v.at[1, k, 5], unit_sem.at[k, 5])
             arrive(cross_v.at[k, 1], cross_sem.at[k])
-        low = both_v[k, x] + decode(cross_v[k, 1]) * unit_v[1, k, 4][:1, :1]
+        low = both_v[k, x] + decode(cross_v[k, 1]) * unit_v[1, k, 5][:1, :1]
         lows.append(low)
         squares = squares + jnp.sum(low * low)
     square_v[0] = jnp.full(square_v.shape[1:], squares, jnp.float32)
@@ -499,7 +521,13 @@
 
                 @pl.when(outer)
                 def _():
-                    wait_bytes(ref.at[k, pl.ds(0, 6)], out_sem.at[out, k])
+                    wait_bytes(ref.at[k, pl.ds(0, 5 if (out, k) in SHIFTED else 6)], out_sem.at[out, k])
+
+                if (out, k) in SHIFTED:
+
+                    @pl.when(inner)
+                    def _():
+                        wait_bytes(ref.at[k, 0], out_sem.at[SHIFT + (out == ROWS), k])
 
             wait_bytes(coord_v.at[k, pl.ds(0, m - 1)], out_sem.at[COORD, k])
             wait_bytes(wide_v.at[k, pl.ds(0, m - 1)], out_sem.at[WIDE, k])
@@ -556,21 +584,21 @@
             pltpu.VMEM((2, m, 2, part, tokens), bf16),
             pltpu.VMEM((2, n // 2, 2 * low_rows, columns), f32),
             pltpu.VMEM((2, n // 2, 2 * low_rows, columns), bf16),
-            pltpu.VMEM((2, 2, 2 * low_rows, columns), bf16),
-            pltpu.VMEM((2, 4, 2 * low_rows, columns), bf16),
+            pltpu.VMEM((2, 3, 2 * low_rows, columns), bf16),
+            pltpu.VMEM((2, 5, 2 * low_rows, columns), bf16),
             pltpu.VMEM((2, 2, low_rows, columns), f32),
             pltpu.VMEM((2, 2, low_rows, columns), bf16),
-            pltpu.VMEM((2, 2, 5, 1, 128), f32),
+            pltpu.VMEM((2, 2, 6, 1, 128), f32),
             pltpu.VMEM((n * m, 1, 128), f32),
             pltpu.VMEM((2, n, low_rows, columns), bf16),
             dma((6, 2)),
-            dma((9, 2)),
+            dma((11, 2)),
             dma,
             dma((2,)),
             dma((2, n)),
-            dma((2, 4)),
+            dma((2, 5)),
             dma((2,)),
-            dma((2, 5)),
+            dma((2, 6)),
             dma((2, n)),
             dma((2, n - 1, PIECES)),
             dma((2, 3)),

time: 116 us -> 115 us (level)
    pallas_call x1, Pallas kernels: 111 us -> 109 us  [fused_per_device(): pl.pallas_call(functools.partial(ring_kernel, n, m), out_shape=tuple((plt...]
where the time goes in v4:
time: 115 us
  Pallas kernels  114 us (99%)
    pallas_call x1, Pallas kernels, fused_per_device(): pl.pallas_call(functools.partial(ring_kernel, n, m), out_shape=tuple((plt...  109 us
    pallas_call x1, Pallas kernels, fused_per_device(): pl.pallas_call(functools.partial(write_kernel, len(kinds)), out_shape=tup...  4.69 us

profile of v4, /device:TPU:0, one launch (start us, length us, event | category | flops | bytes accessed | tf_op | source)
XLA Modules:
  0.0 115.0 jit_solution(7680090735200591256)
XLA Ops:
  0.6 109.5 %shard_map.195 = (f32[512,512]{1,0:T(8,128)S(1)}, f32[512,512]{1,0:T(8,128)S(1)}, f32[512,512]{1,0:T(8,128)S(1)}, f32[512,512]{1,0:T(8,128)S(1)}, f32[32,512]{1,...) custom-call(bf16[256,4096]{1,0:T(8,128)(2,1)} %refs_0_.1, ...), custom_call_target="tpu_custom_call" | custom-call | tf_op jit(solution)/shard_map/pallas_call | solution.py:567
  110.2 4.7 %shard_map.196 = (f32[512,512]{1,0:T(8,128)}, f32[512,512]{1,0:T(8,128)}, f32[512,512]{1,0:T(8,128)}, f32[512,512]{1,0:T(8,128)}, f32[32,512]{1,0:T(8,128)}, /*i...) custom-call(f32[512,512]{1,0:T(8,128)S(1)} %get-tuple-element.20.ref, ...), custom_call_target="tpu_custom_call" | custom-call | tf_op jit(solution)/shard_map/pallas_call | solution.py:610

commit v5 on v4

--- a/solution.py
+++ b/solution.py
@@ -148,7 +148,7 @@
         x_v, cot_v, basis, master_v, first, second,
         rows_v, code_v, plain_v, wide_v, flat_v, coord_v, part_v, mine_v, sum_v, got_v, both_v, cross_v, unit_v,
         square_v, direction_v,
-        in_sem, out_sem, square_sem, coord_sem, rows_sem, got_sem, cross_sem, unit_sem, direction_sem, ring_sem, wide_sem,
+        in_sem, out_sem, square_sem, coord_sem, rows_sem, got_sem, cross_sem, unit_sem, ring_sem, wide_sem,
     ) = refs[22:]
     f, t = lax.axis_index("fs"), lax.axis_index("tp")
     me = f * m + t
@@ -276,6 +276,8 @@
         (s, g * FLIGHT + w) for g in range(PIECES // FLIGHT) for s in range(n) for w in range(FLIGHT)
     ]
     arrived, fresh = [], []
+    slot_of, waited, spare = {}, ([], []), ([], [])
+    fresh_slot = {(s, k, c): i for i, (s, c) in enumerate(slots) if s < n - 1 for k in range(2)}
 
     def advance(count, relaxed=True):
         for _ in range(min(count, len(slots))):
@@ -284,9 +286,12 @@
                 if s > 0:
                     with jax.named_scope(f"ring_wait#s={s}#c={c}#k={k}"):
                         ring[s - 1, k, c].wait_recv()
+                        waited[k].append(slot_of[s - 1, k, c])
                 if s < n - 1:
                     where = code_v.at[k, origin[s][k], pl.ds(c * piece, piece)]
-                    ring[s, k, c] = send(where, where, (RING, k), ring_sem.at[k, s, c], {"fs": toward[k]})
+                    slot = spare[k].pop(0) if spare[k] else fresh_slot.pop((s, k, c))
+                    slot_of[s, k, c] = slot
+                    ring[s, k, c] = send(where, where, (RING, k), ring_sem.at[k, slot], {"fs": toward[k]})
             if s > 0:
                 arrived.append((s, c))
                 fresh.append((s, c))
@@ -422,6 +427,7 @@
         low = both_v[k, x] + decode(cross_v[k, 1]) * unit_v[1, k, 5][:1, :1]
         lows.append(low)
         squares = squares + jnp.sum(low * low)
+    settled = [list(indices) for indices in waited]
     square_v[0] = jnp.full(square_v.shape[1:], squares, jnp.float32)
     for d in range(1, n * m):
         other = lax.rem(me + d, n * m)
@@ -440,6 +446,8 @@
         loads["second", k].wait()
     with jax.named_scope("square_wait"):
         wait_bytes(square_v.at[pl.ds(1, n * m - 1)], square_sem)
+    for k in range(2):
+        spare[k].extend(settled[k])
     total_squares = jnp.sum(square_v[...], axis=0)[:1, :1]
     factor = 1.0 / jnp.sqrt(1.0 + total_squares / (2.0 * rank * (columns * m)))
 
@@ -449,15 +457,15 @@
     for k in range(2):
         new_first, new_second, direction = moment_update(lows[k], factor, first[k], second[k])
         direction_v[k, f] = direction
-        push(directions_at(k), DIRECTION, direction_sem, k)
+        push(directions_at(k), DIRECTION, rows_sem, k)
         first_out[k][...] = new_first
         second_out[k][...] = new_second
     advance(pace.pop(0))
     for k in range(2):
-        relay(directions_at(k), DIRECTION, direction_sem, k)
+        relay(directions_at(k), DIRECTION, rows_sem, k)
     advance(pace.pop(0))
     for k in range(2):
-        late(directions_at(k), DIRECTION, direction_sem, k)
+        late(directions_at(k), DIRECTION, rows_sem, k)
 
     def own_rows(k, start, size):
         span = pl.ds(start, size)
@@ -599,8 +607,7 @@
             dma((2, 5)),
             dma((2,)),
             dma((2, 6)),
-            dma((2, n)),
-            dma((2, n - 1, PIECES)),
+            dma((2, min(sum(PACE[:12]), (n - 1) * PIECES))),
             dma((2, 3)),
         ],
         compiler_params=pltpu.CompilerParams(

time: 115 us -> 115 us (level)
  no operation moved by 1% of the time
where the time goes in v5:
time: 115 us
  Pallas kernels  114 us (99%)
    pallas_call x1, Pallas kernels, fused_per_device(): pl.pallas_call(functools.partial(ring_kernel, n, m), out_shape=tuple((plt...  109 us
    pallas_call x1, Pallas kernels, fused_per_device(): pl.pallas_call(functools.partial(write_kernel, len(kinds)), out_shape=tup...  4.69 us

profile of v5, /device:TPU:0, one launch (start us, length us, event | category | flops | bytes accessed | tf_op | source)
XLA Modules:
  0.0 114.6 jit_solution(2700876510814201376)
XLA Ops:
  0.6 109.1 %shard_map.195 = (f32[512,512]{1,0:T(8,128)S(1)}, f32[512,512]{1,0:T(8,128)S(1)}, f32[512,512]{1,0:T(8,128)S(1)}, f32[512,512]{1,0:T(8,128)S(1)}, f32[32,512]{1,...) custom-call(bf16[256,4096]{1,0:T(8,128)(2,1)} %refs_0_.1, ...), custom_call_target="tpu_custom_call" | custom-call | tf_op jit(solution)/shard_map/pallas_call | solution.py:575
  109.7 4.7 %shard_map.196 = (f32[512,512]{1,0:T(8,128)}, f32[512,512]{1,0:T(8,128)}, f32[512,512]{1,0:T(8,128)}, f32[512,512]{1,0:T(8,128)}, f32[32,512]{1,0:T(8,128)}, /*i...) custom-call(f32[512,512]{1,0:T(8,128)S(1)} %get-tuple-element.20.ref, ...), custom_call_target="tpu_custom_call" | custom-call | tf_op jit(solution)/shard_map/pallas_call | solution.py:617
